TPU v7x, 512 devices: a whole 4x8x8 slice. The times are simulated.
512 devices in a mesh: fs: 64 (over z, y), tp: 8 (over x, core).
Axes of the slice: x: 4, y: 8, z: 8, core: 2. Of those that a mesh axis runs over, the one named last changes fastest.
Arguments:
- saved_inputs: bfloat16 [49152, 2048], P('fs'), may hold values from -16 to 16
- cotangents: bfloat16 [3, 49152, 1024], P(None, 'fs', 'tp'), may hold values from -0.02734375 to 0.02734375
- left_roots: float32 [3, 2048, 2048], P(None, 'fs'), may hold values from -1 to 2
- right_roots: float32 [3, 1024, 128], P(None, 'tp'), may hold values from -1 to 2
- moments: float32 [3, 2048, 1024], P(None, 'fs', 'tp'), may hold values from -125 to 125
- masters: float32 [3, 2048, 1024], P(None, 'fs', 'tp'), may hold values from -3 to 3
Outputs:
- direction: float32 [3, 2048, 1024], P(None, 'fs', 'tp')
- moments_new: float32 [3, 2048, 1024], P(None, 'fs', 'tp')
- copies: bfloat16 [3, 2048, 1024], P(None, None, 'tp')
All inputs are finite; a program needn't handle non-finite values.
Results may differ from a plain program's by a relative error of at most 0.002.
Values may be sent and summed in bfloat16 or wider, within the bound.
A program may use at most 64 MiB of HBM per device.

v0:
```python
import jax
import jax.numpy as jnp
from jax import lax
from jax.sharding import Mesh
from jax.sharding import PartitionSpec as P

D = 2048
SBW = 1024
RB = 128
FS = ("fs_0", "fs_1")
TP = ("tp_0", "tp_1")


momentum_decay = 0.9
step_rate = 0.1
eps_value = 1e-06


def filled_up(lines, peers):
    spare = -len(lines) % peers
    return jnp.pad(lines, [(0, spare)] + [(0, 0)] * (lines.ndim - 1))


def in_order(pieces, dim):
    lengths = list(pieces.shape[1:])
    lengths[dim] *= pieces.shape[0]
    return jnp.moveaxis(pieces, 0, dim).reshape(lengths)


def from_everyone(value, axis):
    peers = lax.axis_size(axis)
    return lax.all_to_all(
        jnp.broadcast_to(value[None], (peers, *value.shape)), axis, 0, 0, tiled=True
    )


def collect(value, axis, dim):
    return in_order(from_everyone(value, axis), dim)


def in_blocks(value, dim, peers):
    before, after = (value.shape[:dim], value.shape[dim + 1 :])
    return jnp.moveaxis(value.reshape(*before, peers, -1, *after), dim, 0)


def summed_on_arrival(value, axis, dim):
    peers = lax.axis_size(axis)
    pieces = lax.all_to_all(in_blocks(value, dim, peers), axis, 0, 0, tiled=True)
    return jnp.sum(pieces.astype(jnp.float32), axis=0)


def nested_sum(value, axes):
    lines = value.reshape(-1, value.shape[-1])
    padded = filled_up(lines, lax.axis_size(axes))
    whole = collect(summed_on_arrival(padded, axes, 0).astype(jnp.bfloat16), axes, 0)
    return lax.slice_in_dim(whole, 0, len(lines)).reshape(value.shape).astype(jnp.float32)


def taken_together(value, axis):
    everything = from_everyone(value, axis)
    return jnp.sum(everything, axis=0)


def by_axis(value, axes):
    far, near = axes
    nearer = taken_together(value, near)
    return taken_together(nearer, far)


def on_device(saved_inputs, cotangents, left_roots, right_roots, moments, masters):
    rows_own = masters.shape[1]
    columns = masters.shape[2]
    partial_value = jnp.einsum(
        "td,mtc->dmc", saved_inputs, cotangents, preferred_element_type=jnp.float32
    )
    summed = nested_sum(partial_value.astype(jnp.bfloat16), FS)
    left_done = jnp.einsum("mrd,dmc->mrc", left_roots, summed, precision=lax.Precision.HIGHEST)
    block_count = columns // RB
    right_blocks = right_roots.reshape(3, block_count, RB, RB)
    right_done = jnp.einsum(
        "mrbi,mbij->mrbj",
        left_done.reshape(3, rows_own, block_count, RB),
        right_blocks,
        precision=lax.Precision.HIGHEST,
    ).reshape(3, rows_own, columns)
    moments_new = momentum_decay * moments + right_done
    totals = by_axis(
        jnp.sum(moments_new * moments_new, axis=(1, 2)), (("fs_0", "fs_1"), ("tp_0", "tp_1"))
    )
    meansq = totals / (D * SBW)
    direction = moments_new * lax.rsqrt(meansq + eps_value)[:, None, None]
    copy_rows = (masters - step_rate * direction).astype(jnp.bfloat16)
    copies = lax.all_gather(copy_rows, FS, axis=1, tiled=True)
    return (direction, moments_new, copies)


def solution(mesh):
    torus = Mesh(mesh.devices.reshape(8, 8, 4, 2), ("fs_0", "fs_1", "tp_0", "tp_1"))
    in_specs = (
        P(FS, None),
        P(None, FS, TP),
        P(None, FS, None),
        P(None, TP, None),
        P(None, FS, TP),
        P(None, FS, TP),
    )
    out_specs = (P(None, FS, TP), P(None, FS, TP), P(None, None, TP))
    return jax.shard_map(
        on_device, mesh=torus, in_specs=in_specs, out_specs=out_specs, check_vma=False
    )
```

profile of v0, /device:TPU:1, one launch (start us, length us, event | category | flops | bytes accessed | tf_op | source)
XLA Modules:
  0.0 248.1 jit_solution(6863095140001499343)
XLA Ops:
  7.2 0.0 copy-start
  7.2 0.0 all-gather.2.cloned.1.call-start
  7.2 1.8 copy-done
  9.1 2.9 %fusion.2 = bf16[2048,3,128]{2,0,1:T(8,128)(2,1)S(1)} fusion(bf16[3,768,128]{2,1,0:T(8,128)(2,1)} %param.7, bf16[768,2048]{1,0:T(8,128)(2,1)S(1)} %copy-done), kind=kOutput, calls=%fused_computation.2 | convolution fusion | flops 1208745984 | bytes 5308416 | tf_op jit(solution)/shard_map/td,mtc->dmc/dot_general | solution.py:73
  12.0 10.8 %copy.21 = bf16[2048,3,128]{2,1,0:T(4,128)(2,1)} copy(bf16[2048,3,128]{2,0,1:T(8,128)(2,1)S(1)} %fusion.2) | data formatting | bytes 3145728 | tf_op jit(solution)/shard_map/convert_element_type | solution.py:76
  22.8 5.0 %reshape.37 = bf16[64,96,128]{2,1,0:T(8,128)(2,1)} reshape(bf16[2048,3,128]{2,1,0:T(4,128)(2,1)} %copy.21) | data formatting | bytes 3145728 | tf_op jit(solution)/shard_map/reshape | solution.py:43
  27.8 56.3 %all_to_all.22 = bf16[64,96,128]{2,1,0:T(8,128)(2,1)} all-to-all(bf16[64,96,128]{2,1,0:T(8,128)(2,1)} %reshape.37), channel_id=1, replica_groups=mesh['fs_0'=8,'fs_1'=8,'tp_0'=4,'tp_1'=2] {'fs_0','fs_1'}, dimensions={0} | all-to-all | bytes 3145728 | tf_op jit(solution)/shard_map/all_to_all | solution.py:48
  84.1 1.7 reduce_sum.39
  85.7 0.2 broadcast_in_dim.6
  85.9 45.8 %all_to_all.23 = bf16[64,96,128]{2,1,0:T(8,128)(2,1)} all-to-all(bf16[64,96,128]{2,1,0:T(8,128)(2,1)S(1)} %broadcast_in_dim.6), channel_id=1, replica_groups=mesh['fs_0'=8,'fs_1'=8,'tp_0'=4,'tp_1'=2] {'fs_0','fs_1'}, dimensions={0} | all-to-all | bytes 3145728 | tf_op jit(solution)/shard_map/all_to_all | solution.py:32
  131.7 5.2 %reshape_reshape.3 = bf16[2048,3,128]{2,1,0:T(4,128)(2,1)} reshape(bf16[64,96,128]{2,1,0:T(8,128)(2,1)} %all_to_all.23) | data formatting | bytes 3145728 | tf_op jit(solution)/shard_map/reshape;reshape | solution.py:56
  136.9 2.6 %fusion.5 = f32[3,128,32]{1,2,0:T(8,128)S(1)} fusion(f32[3,32,2048]{2,1,0:T(8,128)} %param.8, bf16[2048,3,128]{2,1,0:T(4,128)(2,1)} %reshape_reshape.3), kind=kOutput, calls=%fused_computation.3 | convolution fusion | flops 301989888 | bytes 2408448 | tf_op jit(solution)/shard_map/mrd,dmc->mrc/dot_general | solution.py:77
  139.6 0.0 copy-done.1
  139.6 0.0 copy-done.4
  139.6 0.4 multiply_reduce_fusion
  140.0 13.4 %all_to_all.24 = f32[8,1,3]{2,1,0:T(1,128)S(1)} all-to-all(f32[8,1,3]{2,1,0:T(1,128)S(1)} %broadcast_in_dim.7), channel_id=1, replica_groups=mesh['fs_0'=8,'fs_1'=8,'tp_0'=4,'tp_1'=2] {'tp_0','tp_1'}, dimensions={0} | all-to-all | bytes 192 | tf_op jit(solution)/shard_map/all_to_all | solution.py:32
  153.4 17.1 %all_to_all.25 = f32[64,1,3]{2,1,0:T(1,128)S(1)} all-to-all(f32[64,1,3]{2,1,0:T(1,128)S(1)} %broadcast_in_dim.8), channel_id=1, replica_groups=mesh['fs_0'=8,'fs_1'=8,'tp_0'=4,'tp_1'=2] {'fs_0','fs_1'}, dimensions={0} | all-to-all | bytes 1536 | tf_op jit(solution)/shard_map/all_to_all | solution.py:32
  170.5 0.1 reduce_sum.42
  170.6 0.0 copy-done.3
  170.6 0.7 subtract_convert_fusion
  171.3 0.0 all-gather.2.cloned.1.call-update
  171.3 67.2 %all-gather.2.cloned.1.call-done = bf16[3,2048,128]{2,1,0:T(8,128)(2,1)} async-done(((bf16[3,32,128]{2,1,0:T(8,128)(2,1)}), bf16[3,2048,128]{2,1,0:T(8,128)(2,1)}) %all-gather.2.cloned.1.call-update) | async-done | bytes 1572880 | tf_op jit(solution)/shard_map/all_gather | solution.py:93
  238.6 2.7 %copy.32 = bf16[3,2048,128]{2,1,0:T(8,128)(2,1)} copy(bf16[3,2048,128]{2,1,0:T(8,128)(2,1)} %all-gather.2.cloned.1.call-done) | data formatting | bytes 3145728
  241.2 0.0 copy-done.2
  (8 shorter events, 0.1 us)
Async XLA Ops:
  7.2 1.9 copy-start
  7.2 231.4 %all-gather.2.cloned.1.call-start = ((), (), s32[]{:S(2)}) async-start(), calls=%async_computation.4 | async-start | bytes 1597440 | tf_op jit(solution)/shard_map/all_gather | solution.py:93
  136.9 2.6 %copy-start.1 = (f32[3,128,128]{2,1,0:T(8,128)S(1)}, f32[3,128,128]{2,1,0:T(8,128)}, u32[]{:S(2)}) copy-start(f32[3,128,128]{2,1,0:T(8,128)} %param.9) | copy-start | bytes 589828
  136.9 2.7 %copy-start.4 = (f32[3,32,128]{2,1,0:T(8,128)S(1)}, f32[3,32,128]{2,1,0:T(8,128)}, u32[]{:S(2)}) copy-start(f32[3,32,128]{2,1,0:T(8,128)} %param.10) | copy-start | bytes 147460
  136.9 33.7 %copy-start.3 = (f32[3,32,128]{2,1,0:T(8,128)S(1)}, f32[3,32,128]{2,1,0:T(8,128)}, u32[]{:S(2)}) copy-start(f32[3,32,128]{2,1,0:T(8,128)} %param.11) | copy-start | bytes 147460
  140.0 101.2 %copy-start.2 = (f32[3,32,128]{2,1,0:T(8,128)}, f32[3,32,128]{2,1,0:T(8,128)S(1)}, u32[]{:S(2)}) copy-start(f32[3,32,128]{2,1,0:T(8,128)S(1)} %get-tuple-element.11) | copy-start | bytes 147460
Sparse Core Ops, SparseCore 0:
  171.4 67.0 all-gather.1
where the time goes:
time: 253 us; the launch traced here: 248 us
  blocking collectives  133 us (53%)
  waiting for transfers between devices  67.3 us (27%)
  local copies, waits for them, and re-layouts  25.7 us (10%)
  between operations  14.1 us (6%)
  matrix products  5.91 us (2%)
    all_to_all x3, blocking collectives, from_everyone(): lax.all_to_all(jnp.broadcast_to(value[None], (peers, *value.shape)), axis...  76.3 us
    all_gather x1, waiting for transfers between devices, on_device(): copies = lax.all_gather(copy_rows, FS, axis=1, tiled=True)  67.2 us
    all_to_all x1, blocking collectives, summed_on_arrival(): lax.all_to_all(in_blocks(value, dim, peers), axis, 0, 0, tiled=True)  56.3 us
    convert_element_type x1, local copies, waits for them, and re-layouts, on_device(): summed = nested_sum(partial_value.astype(jnp.bfloat16), FS)  10.8 us
    another operation x1, local copies, waits for them, and re-layouts, nested_sum(): lax.slice_in_dim(whole, 0, len(lines)).reshape(value.shape)  5.19 us
  transfers between devices with their start and end apart: 1, of which 1 were waited for; matrix products, arithmetic and copies ran while one was open for 0% of the time, Pallas kernels for 0%

commit v1 on v0

v1 whole, which is shorter than its diff:
```python
import functools

import jax
import jax.numpy as jnp
from jax import lax
from jax.experimental import pallas as pl
from jax.experimental.pallas import tpu as pltpu
from jax.sharding import Mesh
from jax.sharding import PartitionSpec as P

Z, Y, X, CORE = "fs_0", "fs_1", "tp_0", "tp_1"
FS, TP = (Z, Y), (X, CORE)
MESH = pl.DeviceIdType.MESH
F32, BF16 = jnp.float32, jnp.bfloat16
M = 3
W = 128

momentum_decay = 0.9
step_rate = 0.1
eps_value = 1e-06


def far_first(n):
    return sorted(range(1, n), key=lambda o: -min(o, n - o))


def kernel(n, nx, nc, entries, x_hbm, c_hbm, l_hbm, rr_hbm, mo_hbm, ma_hbm,
           dir_hbm, mn_hbm, cp_hbm,
           xs, cv, ct, lv, ls, rr, mo, dirv, mnv, pb, own, rb, s2, g1, r2, gf,
           mal, mnl, sq1, sq2, sq3, cp,
           load_sem, out_sem, send_sem, rb_sem, r2_sem, ag_sem, gf_sem, ma_sem, mnl_sem,
           sq_sem1, sq_sem2, sq_sem3, cp_sem):
    z, y = lax.axis_index(Z), lax.axis_index(Y)
    x, core = lax.axis_index(X), lax.axis_index(CORE)
    nt = nx * nc
    t = x * nc + core
    c16 = W // n
    half = n // 2
    hr = mal.shape[3]
    big = ((Y, y), (Z, z))
    small = ((Z, z), (Y, y))
    sgn = 1 - 2 * core

    def at(i):
        return lax.rem(i + 2 * n, n)

    def remote(src, dst, ssem, rsem, where):
        return pltpu.make_async_remote_copy(
            src_ref=src, dst_ref=dst, send_sem=ssem, recv_sem=rsem,
            device_id=where, device_id_type=MESH)

    def got(dst, sem):
        pltpu.make_async_copy(dst, dst, sem).wait()

    barrier = pltpu.get_barrier_semaphore()

    order = []
    for k in range(half, 0, -1):
        order.append(("L", k))
        if k > 1:
            order.append(("S", k - 1))
    order.append(("O", 0))

    def block_of(h, kind, k):
        b = big[h][1]
        return at(b + sgn * k) if kind == "L" else at(b - sgn * k)

    def load(i, src, dst):
        copy = pltpu.make_async_copy(src, dst, load_sem.at[i])
        copy.start()
        return copy

    c_load = load(0, c_hbm, cv)
    x_loads = []
    for j, (kind, k) in enumerate(order):
        for h in range(2):
            col = pl.multiple_of(h * n * W + block_of(h, kind, k) * W, W)
            x_loads.append(load(1 + 2 * j + h, x_hbm.at[:, pl.ds(col, W)], xs.at[h, j]))
    base = 1 + 2 * n
    ma_loads = [load(base + h, ma_hbm.at[:, pl.ds(h * hr, hr), :],
                     mal.at[h, small[h][1]]) for h in range(2)]
    l_load = load(base + 2, l_hbm, lv)
    rr_load = load(base + 3, rr_hbm, rr)
    mo_load = load(base + 4, mo_hbm, mo)

    for name, me in ((Y, y), (Z, z)):
        for o in range(1, n):
            pl.semaphore_signal(barrier, inc=1, device_id={name: at(me + o)}, device_id_type=MESH)
    for o in range(1, nt):
        q = lax.rem(t + o, nt)
        pl.semaphore_signal(barrier, inc=1, device_id={X: q // nc, CORE: lax.rem(q, nc)},
                            device_id_type=MESH)

    c_load.wait()
    for m in range(M):
        ct[m * W:(m + 1) * W, :] = cv[m].T

    def ring_to(h, chain):
        name, b = big[h]
        return {name: at(b + sgn) if chain == "L" else at(b - sgn)}

    def slot(chain, s):
        return s - 1 if chain == "L" else half + s - 1

    def send_sum(h, chain, s, m):
        k = half + 1 - s if chain == "L" else half - s
        src = pb.at[h, block_of(h, chain, k), m]
        i = slot(chain, s)
        remote(src, rb.at[h, i, m], send_sem.at[0], rb_sem.at[h, i, m], ring_to(h, chain)).start()

    waited = False
    for j, (kind, k) in enumerate(order):
        for h in range(2):
            x_loads[2 * j + h].wait()
        both = jnp.concatenate([xs[0, j], xs[1, j]], axis=1)
        part = jnp.dot(ct[...], both, preferred_element_type=F32)
        for h in range(2):
            for m in range(M):
                piece = part[m * W:(m + 1) * W, h * W:(h + 1) * W]
                if kind == "O":
                    own[h, m] = piece
                else:
                    pb[h, block_of(h, kind, k), m] = piece.astype(BF16)
        if j == 0:
            pl.semaphore_wait(barrier, 2 * (n - 1) + nt - 1)
        if (kind, k) == ("L", half) or (kind, k) == ("S", half - 1):
            for m in range(M):
                for h in range(2):
                    send_sum(h, kind, 1, m)

    for h in range(2):
        ma_loads[h].wait()

    for s in range(2, half + 1):
        for m in range(M):
            for chain, last in (("L", half), ("S", half - 1)):
                if s > last:
                    continue
                k = half + 1 - s if chain == "L" else half - s
                for h in range(2):
                    i = slot(chain, s - 1)
                    got(rb.at[h, i, m], rb_sem.at[h, i, m])
                    b = block_of(h, chain, k)
                    pb[h, b, m] = (pb[h, b, m].astype(F32) + rb[h, i, m].astype(F32)).astype(BF16)
                    send_sum(h, chain, s, m)

    for m in range(M):
        for h in range(2):
            total = own[h, m]
            for chain, last in (("S", half - 1), ("L", half)):
                if last > 0:
                    i = slot(chain, last)
                    got(rb.at[h, i, m], rb_sem.at[h, i, m])
                    total = total + rb[h, i, m].astype(F32)
            g1[h, m] = total
            s2[h, m] = total.astype(BF16)

    peers = far_first(n)
    for o in peers:
        for h in range(2):
            name, me = small[h]
            q = at(me + o)
            rows = pl.ds(pl.multiple_of(q * c16, c16), c16)
            remote(s2.at[h, :, rows, :], r2.at[h, o - 1], send_sem.at[1], r2_sem.at[h, o - 1],
                   {name: q}).start()
    l_load.wait()
    rows_own = lv.shape[1]
    for m in range(M):
        value = lv[m]
        high = value.astype(BF16)
        ls[m, 0:rows_own, :] = high
        ls[m, rows_own:2 * rows_own, :] = (value - high.astype(F32)).astype(BF16)

    for h in range(2):
        name, me = small[h]
        rows = pl.ds(pl.multiple_of(me * c16, c16), c16)
        b = big[h][1]
        total = g1[h, :, rows, :]
        for o in range(1, n):
            got(r2.at[h, o - 1], r2_sem.at[h, o - 1])
            total = total + r2[h, o - 1].astype(F32)
        gf[h, b, :, rows, :] = total.astype(BF16)
        for o in peers:
            mine = gf.at[h, b, :, rows, :]
            remote(mine, mine, send_sem.at[2], ag_sem.at[h, o - 1], {name: at(me + o)}).start()

    for h in range(2):
        name, me = small[h]
        for o in peers:
            mine = mal.at[h, me]
            remote(mine, mine, send_sem.at[3], ma_sem.at[h, o - 1], {name: at(me + o)}).start()

    for h in range(2):
        name, me = small[h]
        for o in range(1, n):
            rows = pl.ds(pl.multiple_of(at(me - o) * c16, c16), c16)
            got(gf.at[h, big[h][1], :, rows, :], ag_sem.at[h, o - 1])

    def held(h, chain, s):
        b = big[h][1]
        return at(b - sgn * s) if chain == "L" else at(b + sgn * s)

    acc = [jnp.zeros((2 * rows_own, W), F32) for _ in range(M)]

    def add_block(h, b, m):
        cols = pl.ds(pl.multiple_of(h * n * W + b * W, W), W)
        acc[m] = acc[m] + lax.dot_general(
            ls[m, :, cols], gf[h, b, m], (((1,), (1,)), ((), ())), preferred_element_type=F32)

    def send_block(buffer, index, h, chain, s, m, number, sems):
        ref = index(buffer, h, held(h, chain, s - 1), m)
        remote(ref, ref, send_sem.at[number + h], sems.at[h, slot(chain, s), m], ring_to(h, chain)).start()

    def g_index(buffer, h, b, m):
        return buffer.at[h, b, m]

    def ring_gather(buffer, index, number, sems, arrived):
        for m in range(M):
            for h in range(2):
                for chain, last in (("L", half), ("S", half - 1)):
                    if last > 0:
                        send_block(buffer, index, h, chain, 1, m, number, sems)
        for m in range(M):
            for h in range(2):
                arrived(h, big[h][1], m)
        for s in range(1, half + 1):
            for m in range(M):
                came = []
                for chain, last in (("L", half), ("S", half - 1)):
                    if s > last:
                        continue
                    for h in range(2):
                        b = held(h, chain, s)
                        got(index(buffer, h, b, m), sems.at[h, slot(chain, s), m])
                        if s < last:
                            send_block(buffer, index, h, chain, s + 1, m, number, sems)
                        came.append((h, b))
                for h, b in came:
                    arrived(h, b, m)

    ring_gather(gf, g_index, 9, gf_sem, add_block)

    rr_load.wait()
    mo_load.wait()
    sums = []
    for m in range(M):
        left = acc[m][0:rows_own] + acc[m][rows_own:2 * rows_own]
        right = jnp.dot(left, rr[m], precision=lax.Precision.HIGHEST, preferred_element_type=F32)
        new = momentum_decay * mo[m] + right
        mnv[m] = new
        for h in range(2):
            mnl[h, small[h][1], m] = new[h * hr:(h + 1) * hr]
        sums.append(jnp.sum(new * new, axis=0, keepdims=True))
    sq1[y] = jnp.concatenate(sums + [jnp.zeros((8 - M, W), F32)], axis=0)

    for o in peers:
        remote(sq1.at[y], sq1.at[y], send_sem.at[5], sq_sem1.at[o - 1], {Y: at(y + o)}).start()
    out_copies = [pltpu.make_async_copy(mnv, mn_hbm, out_sem.at[0])]
    out_copies[0].start()
    for h in range(2):
        name, me = small[h]
        for o in peers:
            mine = mnl.at[h, me]
            remote(mine, mine, send_sem.at[6], mnl_sem.at[h, o - 1], {name: at(me + o)}).start()

    def summed(ref, count):
        total = ref[0]
        for i in range(1, count):
            total = total + ref[i]
        return total

    for o in range(1, n):
        got(sq1.at[at(y - o)], sq_sem1.at[o - 1])
    sq2[z] = summed(sq1, n)
    for o in peers:
        remote(sq2.at[z], sq2.at[z], send_sem.at[4], sq_sem2.at[o - 1], {Z: at(z + o)}).start()
    for o in range(1, n):
        got(sq2.at[at(z - o)], sq_sem2.at[o - 1])
    sq3[t] = summed(sq2, n)
    for o in range(1, nt):
        q = lax.rem(t + o, nt)
        remote(sq3.at[t], sq3.at[t], send_sem.at[7], sq_sem3.at[o - 1],
               {X: q // nc, CORE: lax.rem(q, nc)}).start()
    for h in range(2):
        name, me = small[h]
        for o in range(1, n):
            got(mal.at[h, at(me - o)], ma_sem.at[h, o - 1])
            got(mnl.at[h, at(me - o)], mnl_sem.at[h, o - 1])
    for o in range(1, nt):
        got(sq3.at[lax.rem(t - o + nt, nt)], sq_sem3.at[o - 1])
    totals = jnp.sum(summed(sq3, nt), axis=1, keepdims=True)
    scales = lax.rsqrt(totals / entries + eps_value)

    def c_index(buffer, h, b, m):
        return buffer.at[m, :, b, 0] if h == 0 else buffer.at[m, b, :, 1]

    for m in range(M):
        scale = scales[m:m + 1, :]
        for h in range(2):
            for i in range(n):
                value = (mal[h, i, m] - step_rate * (mnl[h, i, m] * scale)).astype(BF16)
                if h == 0:
                    cp[m, i, y, 0] = value
                else:
                    cp[m, z, i, 1] = value

    def put_out(h, b, m):
        pass

    ring_gather(cp, c_index, 11, cp_sem, put_out)
    for m in range(M):
        dirv[m] = mnv[m] * scales[m:m + 1, :]
    out_copies.append(pltpu.make_async_copy(dirv, dir_hbm, out_sem.at[1]))
    out_copies[1].start()
    out_copies.append(pltpu.make_async_copy(cp, cp_hbm, out_sem.at[2]))
    out_copies[2].start()

    got(rb, send_sem.at[0])
    got(r2, send_sem.at[1])
    got(r2, send_sem.at[2])
    for number, buffer in ((3, mal), (6, mnl)):
        got(buffer.at[:, 0:n - 1], send_sem.at[number])
    got(gf.at[0, 0:n - 1], send_sem.at[9])
    got(gf.at[1, 0:n - 1], send_sem.at[10])
    got(sq1.at[0:n - 1], send_sem.at[5])
    got(sq2.at[0:n - 1], send_sem.at[4])
    if nt > 1:
        got(sq3.at[0:nt - 1], send_sem.at[7])
    got(cp.at[:, 0:n - 1, :, 0], send_sem.at[11])
    got(cp.at[:, 0:n - 1, :, 1], send_sem.at[12])
    for copy in out_copies:
        copy.wait()


def update(n, nx, nc, x, c, l, rr, mo, ma):
    tokens, depth = x.shape
    rows_own = l.shape[1]
    hr = rows_own // 2
    c16 = W // n
    vmem, dma = pltpu.VMEM, pltpu.SemaphoreType.DMA
    nt = nx * nc
    peers = max(n - 1, 1)
    scratch = [
        vmem((2, n, tokens, W), BF16),
        vmem((M, tokens, W), BF16),
        vmem((M * W, tokens), BF16),
        vmem((M, rows_own, depth), F32),
        vmem((M, 2 * rows_own, depth), BF16),
        vmem((M, W, W), F32),
        vmem((M, rows_own, W), F32),
        vmem((M, rows_own, W), F32),
        vmem((M, rows_own, W), F32),
        vmem((2, n, M, W, W), BF16),
        vmem((2, M, W, W), F32),
        vmem((2, n - 1, M, W, W), BF16),
        vmem((2, M, W, W), BF16),
        vmem((2, M, W, W), F32),
        vmem((2, n - 1, M, c16, W), BF16),
        vmem((2, n, M, W, W), BF16),
        vmem((2, n, M, hr, W), F32),
        vmem((2, n, M, hr, W), F32),
        vmem((n, 8, W), F32),
        vmem((n, 8, W), F32),
        vmem((nt, 8, W), F32),
        vmem((M, n, n, 2, hr, W), BF16),
        dma((1 + 2 * n + 5,)),
        dma((3,)),
        dma((13,)),
        dma((2, n - 1, M)),
        dma((2, n - 1)),
        dma((2, n - 1)),
        dma((2, n - 1, M)),
        dma((2, n - 1)),
        dma((2, n - 1)),
        dma((peers,)), dma((peers,)), dma((max(nt - 1, 1),)),
        dma((2, n - 1, M)),
    ]
    small = jax.ShapeDtypeStruct((M, rows_own, W), F32)
    any_ = pl.BlockSpec(memory_space=pl.ANY)
    direction, new, copies = pl.pallas_call(
        functools.partial(kernel, n, nx, nc, float(depth * W * nt)),
        out_shape=(small, small, jax.ShapeDtypeStruct((M, n, n, 2, hr, W), BF16)),
        in_specs=[any_] * 6,
        out_specs=(any_,) * 3,
        scratch_shapes=scratch,
        name="update",
        compiler_params=pltpu.CompilerParams(
            collective_id=0, has_side_effects=True, vmem_limit_bytes=60 * 1024 * 1024),
    )(x, c, l, rr, mo, ma)
    return direction, new, copies.reshape(M, n * n * rows_own, W)


def solution(mesh):
    n, nx, nc = 8, 4, 2
    torus = Mesh(mesh.devices.reshape(n, n, nx, nc), (Z, Y, X, CORE))
    in_specs = (
        P(FS, None),
        P(None, FS, TP),
        P(None, FS, None),
        P(None, TP, None),
        P(None, FS, TP),
        P(None, FS, TP),
    )
    out_specs = (P(None, FS, TP), P(None, FS, TP), P(None, None, TP))
    return jax.shard_map(
        functools.partial(update, n, nx, nc),
        mesh=torus, in_specs=in_specs, out_specs=out_specs, check_vma=False)
```

time: 253 us -> 95.5 us (0.38)
  the two profiles are of different devices: /device:TPU:1 before, /device:TPU:2 now
where the time goes in v1:
time: 95.5 us; the launch traced here: 95.2 us
  Pallas kernels  89.1 us (93%)
  local copies, waits for them, and re-layouts  5.49 us (6%)
    pallas_call x1, Pallas kernels, update(): pl.pallas_call(functools.partial(kernel, n, nx, nc, float(depth * W * nt)...  89.1 us
    unnamed x3, local copies, waits for them, and re-layouts  5.49 us

profile of v1, /device:TPU:2, one launch (start us, length us, event | category | flops | bytes accessed | tf_op | source)
XLA Modules:
  0.0 95.2 jit_solution(3791645542052903169)
XLA Ops:
  0.6 89.1 %update.1 = (f32[3,32,128]{2,1,0:T(8,128)}, f32[3,32,128]{2,1,0:T(8,128)}, bf16[3,8,8,2,16,128]{5,4,3,2,1,0:T(8,128)(2,1)}) custom-call(bf16[768,2048]{1,0:T(8,128)(2,1)} %x_hbm.1, bf16[3,768,128]{2,1,0:T(8,128)(2,1)} %c_hbm.1, f32[3,32,2048]{2,1,0:T(8,128)} %l_hbm.1, f32[3,128,128]{2,1,0:T(8,128)} %rr_hbm.1, f32[3,32,128]{2,1,0:T(8,128)} %mo_hbm.1, ...), custom_call_target="tpu_custom_call" | custom-call | tf_op jit(solution)/shard_map/update/pallas_call | solution.py:380
  89.7 1.4 %copy.12 = f32[3,32,128]{2,1,0:T(8,128)} copy(f32[3,32,128]{2,1,0:T(8,128)} %get-tuple-element.12) | data formatting | bytes 98304
  91.1 1.4 %copy.13 = f32[3,32,128]{2,1,0:T(8,128)} copy(f32[3,32,128]{2,1,0:T(8,128)} %get-tuple-element.13) | data formatting | bytes 98304
  92.5 2.7 %copy.14 = bf16[3,2048,128]{2,1,0:T(8,128)(2,1)} copy(bf16[3,2048,128]{2,1,0:T(8,128)(2,1)} %bitcast.1) | data formatting | bytes 3145728

commit v2 on v1

v2 whole, which is shorter than its diff:
```python
import functools

import jax
import jax.numpy as jnp
from jax import lax
from jax.experimental import pallas as pl
from jax.experimental.pallas import tpu as pltpu
from jax.sharding import Mesh
from jax.sharding import PartitionSpec as P

Z, Y, X, CORE = "fs_0", "fs_1", "tp_0", "tp_1"
FS, TP = (Z, Y), (X, CORE)
MESH = pl.DeviceIdType.MESH
F32, BF16 = jnp.float32, jnp.bfloat16
M = 3
W = 128
PARTS = 2

momentum_decay = 0.9
step_rate = 0.1
eps_value = 1e-06


def far_first(n):
    return sorted(range(1, n), key=lambda o: -min(o, n - o))


def kernel(n, nx, nc, entries, x_hbm, c_hbm, l_hbm, rr_hbm, mo_hbm, ma_hbm,
           dirv, mnv, cp,
           xs, cv, ct, lv, ls, rr, mo, pb, own, rb, s2, g1, r2, gf, lt, lp, lr,
           mal, mnl, sq1, sq2, sq3,
           load_sem, send_sem, rb_sem, r2_sem, ag_sem, lt_sem, lx_sem, lr_sem, ma_sem, mnl_sem,
           sq_sem1, sq_sem2, sq_sem3, cp_sem):
    z, y = lax.axis_index(Z), lax.axis_index(Y)
    x, core = lax.axis_index(X), lax.axis_index(CORE)
    nt = nx * nc
    t = x * nc + core
    c16 = W // n
    half = n // 2
    rows_own = lv.shape[1]
    peers = far_first(n)
    hr = mal.shape[3]
    big = ((Y, y), (Z, z))
    small = ((Z, z), (Y, y))
    sgn = 1 - 2 * core

    def at(i):
        return lax.rem(i + 2 * n, n)

    def remote(src, dst, ssem, rsem, where):
        return pltpu.make_async_remote_copy(
            src_ref=src, dst_ref=dst, send_sem=ssem, recv_sem=rsem,
            device_id=where, device_id_type=MESH)

    def got(dst, sem):
        pltpu.make_async_copy(dst, dst, sem).wait()

    barrier = pltpu.get_barrier_semaphore()

    order = []
    for k in range(half, 0, -1):
        order.append(("L", k))
        if k > 1:
            order.append(("S", k - 1))
    order.append(("O", 0))

    def block_of(h, kind, k):
        b = big[h][1]
        return at(b + sgn * k) if kind == "L" else at(b - sgn * k)

    def load(i, src, dst):
        copy = pltpu.make_async_copy(src, dst, load_sem.at[i])
        copy.start()
        return copy

    c_load = load(0, c_hbm, cv)
    x_loads = []
    for j, (kind, k) in enumerate(order):
        for h in range(2):
            col = pl.multiple_of(h * n * W + block_of(h, kind, k) * W, W)
            x_loads.append(load(1 + 2 * j + h, x_hbm.at[:, pl.ds(col, W)], xs.at[h, j]))
    base = 1 + 2 * n
    ma_loads = [load(base + h, ma_hbm.at[:, pl.ds(h * hr, hr), :],
                     mal.at[h, small[h][1]]) for h in range(2)]
    l_load = load(base + 2, l_hbm, lv)
    rr_load = load(base + 3, rr_hbm, rr)
    mo_load = load(base + 4, mo_hbm, mo)

    for name, me in ((Y, y), (Z, z)):
        for o in range(1, n):
            pl.semaphore_signal(barrier, inc=1, device_id={name: at(me + o)}, device_id_type=MESH)
    for o in range(1, nt):
        q = lax.rem(t + o, nt)
        pl.semaphore_signal(barrier, inc=1, device_id={X: q // nc, CORE: lax.rem(q, nc)},
                            device_id_type=MESH)

    c_load.wait()
    for m in range(M):
        ct[m * W:(m + 1) * W, :] = cv[m].T

    def ring_to(h, chain):
        name, b = big[h]
        return {name: at(b + sgn) if chain == "L" else at(b - sgn)}

    def slot(chain, s):
        return s - 1 if chain == "L" else half + s - 1

    cp_rows = W // PARTS

    def send_sum(h, chain, s, m, p):
        k = half + 1 - s if chain == "L" else half - s
        rows = pl.ds(p * cp_rows, cp_rows)
        src = pb.at[h, block_of(h, chain, k), m, rows]
        i = slot(chain, s)
        remote(src, rb.at[h, i, m, rows], send_sem.at[0], rb_sem.at[h, i, m * PARTS + p],
               ring_to(h, chain)).start()

    def got_sum(h, i, m, p):
        rows = pl.ds(p * cp_rows, cp_rows)
        got(rb.at[h, i, m, rows], rb_sem.at[h, i, m * PARTS + p])
        return rb[h, i, m, rows].astype(F32)

    waited = False
    for j, (kind, k) in enumerate(order):
        for h in range(2):
            x_loads[2 * j + h].wait()
        both = jnp.concatenate([xs[0, j], xs[1, j]], axis=1)
        part = jnp.dot(ct[...], both, preferred_element_type=F32)
        for h in range(2):
            for m in range(M):
                piece = part[m * W:(m + 1) * W, h * W:(h + 1) * W]
                if kind == "O":
                    own[h, m] = piece
                else:
                    pb[h, block_of(h, kind, k), m] = piece.astype(BF16)
        if j == 0:
            pl.semaphore_wait(barrier, 2 * (n - 1) + nt - 1)
        if (kind, k) == ("L", half) or (kind, k) == ("S", half - 1):
            for m in range(M):
                for p in range(PARTS):
                    for h in range(2):
                        send_sum(h, kind, 1, m, p)

    share = rows_own // nx
    part_rows = pl.ds(pl.multiple_of(x * share, share), share)
    l_load.wait()
    for o in peers:
        for h in range(2):
            name, me = big[h]
            q = at(me + o)
            cols = pl.ds(pl.multiple_of(h * n * W + q * W, W), W)
            remote(lv.at[:, part_rows, cols], lt.at[h, o - 1, :, part_rows, :], send_sem.at[8],
                   lt_sem.at[h, o - 1], {name: q}).start()

    for s in range(2, half + 1):
        for m in range(M):
            for p in range(PARTS):
                rows = pl.ds(p * cp_rows, cp_rows)
                for chain, last in (("L", half), ("S", half - 1)):
                    if s > last:
                        continue
                    k = half + 1 - s if chain == "L" else half - s
                    for h in range(2):
                        came = got_sum(h, slot(chain, s - 1), m, p)
                        b = block_of(h, chain, k)
                        pb[h, b, m, rows] = (pb[h, b, m, rows].astype(F32) + came).astype(BF16)
                        send_sum(h, chain, s, m, p)

    for m in range(M):
        for p in range(PARTS):
            rows = pl.ds(p * cp_rows, cp_rows)
            for h in range(2):
                total = own[h, m, rows]
                for chain, last in (("S", half - 1), ("L", half)):
                    if last > 0:
                        total = total + got_sum(h, slot(chain, last), m, p)
                g1[h, m, rows] = total
                s2[h, m, rows] = total.astype(BF16)

    for o in peers:
        for h in range(2):
            name, me = small[h]
            q = at(me + o)
            rows = pl.ds(pl.multiple_of(q * c16, c16), c16)
            remote(s2.at[h, :, rows, :], r2.at[h, o - 1], send_sem.at[1], r2_sem.at[h, o - 1],
                   {name: q}).start()
    for h in range(2):
        for o in range(1, n):
            got(lt.at[h, o - 1, :, part_rows, :], lt_sem.at[h, o - 1])
    for o in range(1, nx):
        mine = lt.at[:, :, :, part_rows, :]
        remote(mine, mine, send_sem.at[9], lx_sem.at[o - 1], {X: lax.rem(x + o, nx)}).start()
    for h in range(2):
        name, me = small[h]
        ma_loads[h].wait()
        for o in peers:
            mine = mal.at[h, me]
            remote(mine, mine, send_sem.at[3], ma_sem.at[h, o - 1], {name: at(me + o)}).start()

    def split_left(h, m, o, value):
        high = value.astype(BF16)
        ls[h, m, 2 * o * rows_own:(2 * o + 1) * rows_own, :] = high
        low = (value - high.astype(F32)).astype(BF16)
        ls[h, m, (2 * o + 1) * rows_own:(2 * o + 2) * rows_own, :] = low

    for h in range(2):
        cols = pl.ds(pl.multiple_of(h * n * W + big[h][1] * W, W), W)
        for m in range(M):
            split_left(h, m, 0, lv[m, :, cols])

    for h in range(2):
        name, me = small[h]
        rows = pl.ds(pl.multiple_of(me * c16, c16), c16)
        total = g1[h, :, rows, :]
        for o in range(1, n):
            got(r2.at[h, o - 1], r2_sem.at[h, o - 1])
            total = total + r2[h, o - 1].astype(F32)
        gf[h, :, rows, :] = total.astype(BF16)
        for o in peers:
            mine = gf.at[h, :, rows, :]
            remote(mine, mine, send_sem.at[2], ag_sem.at[h, o - 1], {name: at(me + o)}).start()

    for o in range(1, nx):
        theirs = pl.ds(pl.multiple_of(lax.rem(x + nx - o, nx) * share, share), share)
        got(lt.at[:, :, :, theirs, :], lx_sem.at[o - 1])
    for h in range(2):
        for o in range(1, n):
            for m in range(M):
                split_left(h, m, o, lt[h, o - 1, m])

    left = [jnp.zeros((rows_own, W), F32) for _ in range(M)]
    for h in range(2):
        name, me = small[h]
        for o in range(1, n):
            rows = pl.ds(pl.multiple_of(at(me - o) * c16, c16), c16)
            got(gf.at[h, :, rows, :], ag_sem.at[h, o - 1])
        for m in range(M):
            both = lax.dot_general(ls[h, m], gf[h, m], (((1,), (1,)), ((), ())),
                                   preferred_element_type=F32)
            for o in range(n):
                high = both[2 * o * rows_own:(2 * o + 1) * rows_own]
                value = high + both[(2 * o + 1) * rows_own:(2 * o + 2) * rows_own]
                if o == 0:
                    left[m] = left[m] + value
                else:
                    lp[h, o - 1, m] = value.astype(BF16)
        name, me = big[h]
        for o in peers:
            remote(lp.at[h, o - 1], lr.at[h, o - 1], send_sem.at[10], lr_sem.at[h, o - 1],
                   {name: at(me - o)}).start()
    for h in range(2):
        for o in range(1, n):
            got(lr.at[h, o - 1], lr_sem.at[h, o - 1])
            for m in range(M):
                left[m] = left[m] + lr[h, o - 1, m].astype(F32)

    rr_load.wait()
    mo_load.wait()
    sums = []
    for m in range(M):
        right = jnp.dot(left[m], rr[m], precision=lax.Precision.HIGHEST, preferred_element_type=F32)
        new = momentum_decay * mo[m] + right
        mnv[m] = new
        for h in range(2):
            mnl[h, small[h][1], m] = new[h * hr:(h + 1) * hr]
        sums.append(jnp.sum(new * new, axis=0, keepdims=True))
    sq1[y] = jnp.concatenate(sums + [jnp.zeros((8 - M, W), F32)], axis=0)

    for o in peers:
        remote(sq1.at[y], sq1.at[y], send_sem.at[5], sq_sem1.at[o - 1], {Y: at(y + o)}).start()
    for h in range(2):
        name, me = small[h]
        for o in peers:
            mine = mnl.at[h, me]
            remote(mine, mine, send_sem.at[6], mnl_sem.at[h, o - 1], {name: at(me + o)}).start()

    def summed(ref, count):
        total = ref[0]
        for i in range(1, count):
            total = total + ref[i]
        return total

    for o in range(1, n):
        got(sq1.at[at(y - o)], sq_sem1.at[o - 1])
    sq2[z] = summed(sq1, n)
    for o in peers:
        remote(sq2.at[z], sq2.at[z], send_sem.at[4], sq_sem2.at[o - 1], {Z: at(z + o)}).start()
    for o in range(1, n):
        got(sq2.at[at(z - o)], sq_sem2.at[o - 1])
    sq3[t] = summed(sq2, n)
    for o in range(1, nt):
        q = lax.rem(t + o, nt)
        remote(sq3.at[t], sq3.at[t], send_sem.at[7], sq_sem3.at[o - 1],
               {X: q // nc, CORE: lax.rem(q, nc)}).start()
    for h in range(2):
        name, me = small[h]
        for o in range(1, n):
            got(mal.at[h, at(me - o)], ma_sem.at[h, o - 1])
            got(mnl.at[h, at(me - o)], mnl_sem.at[h, o - 1])
    for o in range(1, nt):
        got(sq3.at[lax.rem(t - o + nt, nt)], sq_sem3.at[o - 1])
    totals = jnp.sum(summed(sq3, nt), axis=1, keepdims=True)
    scales = lax.rsqrt(totals / entries + eps_value)

    def make_copies(h, m, p):
        for i in range(p * lines, (p + 1) * lines):
            scale = scales[m:m + 1, :]
            value = (mal[h, i, m] - step_rate * (mnl[h, i, m] * scale)).astype(BF16)
            if h == 0:
                cp[m, i, y, 0] = value
            else:
                cp[m, z, i, 1] = value

    def held(h, chain, s):
        b = big[h][1]
        return at(b - sgn * s) if chain == "L" else at(b + sgn * s)

    lines = n // PARTS if n >= PARTS else n

    def c_piece(h, b, m, p):
        part = pl.ds(p * lines, lines)
        return cp.at[m, part, b, 0] if h == 0 else cp.at[m, b, part, 1]

    def send_copy(h, chain, s, m, p):
        ref = c_piece(h, held(h, chain, s - 1), m, p)
        remote(ref, ref, send_sem.at[11 + h], cp_sem.at[h, slot(chain, s), m * PARTS + p],
               ring_to(h, chain)).start()

    for m in range(M):
        for p in range(PARTS):
            for h in range(2):
                make_copies(h, m, p)
            for h in range(2):
                send_copy(h, "L", 1, m, p)
                if half > 1:
                    send_copy(h, "S", 1, m, p)
    for m in range(M):
        dirv[m] = mnv[m] * scales[m:m + 1, :]
    for s in range(1, half + 1):
        for m in range(M):
            for p in range(PARTS):
                for chain, last in (("L", half), ("S", half - 1)):
                    if s > last:
                        continue
                    for h in range(2):
                        got(c_piece(h, held(h, chain, s), m, p),
                            cp_sem.at[h, slot(chain, s), m * PARTS + p])
                        if s < last:
                            send_copy(h, chain, s + 1, m, p)

    got(rb, send_sem.at[0])
    got(r2, send_sem.at[1])
    got(r2, send_sem.at[2])
    for number, buffer in ((3, mal), (6, mnl)):
        got(buffer.at[:, 0:n - 1], send_sem.at[number])
    got(lt.at[:, :, :, part_rows, :], send_sem.at[8])
    for o in range(1, nx):
        got(lt.at[:, :, :, pl.ds((o - 1) * share, share), :], send_sem.at[9])
    got(lr, send_sem.at[10])
    got(sq1.at[0:n - 1], send_sem.at[5])
    got(sq2.at[0:n - 1], send_sem.at[4])
    if nt > 1:
        got(sq3.at[0:nt - 1], send_sem.at[7])
    got(cp.at[:, 0:n - 1, :, 0], send_sem.at[11])
    got(cp.at[:, 0:n - 1, :, 1], send_sem.at[12])


def write_out(*refs):
    ins, outs, sem = refs[:3], refs[3:6], refs[6]
    copies = [pltpu.make_async_copy(a, b, sem.at[i]) for i, (a, b) in enumerate(zip(ins, outs))]
    for copy in copies[::-1]:
        copy.start()
    for copy in copies:
        copy.wait()


def update(n, nx, nc, x, c, l, rr, mo, ma):
    tokens, depth = x.shape
    rows_own = l.shape[1]
    hr = rows_own // 2
    c16 = W // n
    vmem, dma = pltpu.VMEM, pltpu.SemaphoreType.DMA
    nt = nx * nc
    peers = max(n - 1, 1)
    scratch = [
        vmem((2, n, tokens, W), BF16),
        vmem((M, tokens, W), BF16),
        vmem((M * W, tokens), BF16),
        vmem((M, rows_own, depth), F32),
        vmem((2, M, 2 * n * rows_own, W), BF16),
        vmem((M, W, W), F32),
        vmem((M, rows_own, W), F32),
        vmem((2, n, M, W, W), BF16),
        vmem((2, M, W, W), F32),
        vmem((2, n - 1, M, W, W), BF16),
        vmem((2, M, W, W), BF16),
        vmem((2, M, W, W), F32),
        vmem((2, n - 1, M, c16, W), BF16),
        vmem((2, M, W, W), BF16),
        vmem((2, n - 1, M, rows_own, W), F32),
        vmem((2, n - 1, M, rows_own, W), BF16),
        vmem((2, n - 1, M, rows_own, W), BF16),
        vmem((2, n, M, hr, W), F32),
        vmem((2, n, M, hr, W), F32),
        vmem((n, 8, W), F32),
        vmem((n, 8, W), F32),
        vmem((nt, 8, W), F32),
        dma((1 + 2 * n + 5,)),
        dma((13,)),
        dma((2, n - 1, M * PARTS)),
        dma((2, n - 1)),
        dma((2, n - 1)),
        dma((2, n - 1)),
        dma((max(nx - 1, 1),)),
        dma((2, n - 1)),
        dma((2, n - 1)),
        dma((2, n - 1)),
        dma((peers,)), dma((peers,)), dma((max(nt - 1, 1),)),
        dma((2, n - 1, M * PARTS)),
    ]
    small = jax.ShapeDtypeStruct((M, rows_own, W), F32)
    any_ = pl.BlockSpec(memory_space=pl.ANY)
    hbm = pl.BlockSpec(memory_space=pltpu.HBM)
    local = pl.BlockSpec(memory_space=pltpu.VMEM)
    shapes = (small, small, jax.ShapeDtypeStruct((M, n, n, 2, hr, W), BF16))
    x, c, l, rr, mo, ma = [pltpu.with_memory_space_constraint(v, pltpu.HBM) for v in (x, c, l, rr, mo, ma)]
    held = pl.pallas_call(
        functools.partial(kernel, n, nx, nc, float(depth * W * nt)),
        out_shape=shapes,
        in_specs=[hbm] * 6,
        out_specs=(local,) * 3,
        scratch_shapes=scratch,
        name="update",
        compiler_params=pltpu.CompilerParams(
            collective_id=0, has_side_effects=True, vmem_limit_bytes=40960 * 1024),
    )(x, c, l, rr, mo, ma)
    direction, new, copies = pl.pallas_call(
        write_out,
        out_shape=shapes,
        in_specs=[local] * 3,
        out_specs=(any_,) * 3,
        scratch_shapes=[dma((3,))],
        name="write_out",
        compiler_params=pltpu.CompilerParams(vmem_limit_bytes=8 * 1024 * 1024),
    )(*held)
    return direction, new, copies.reshape(M, n * n * rows_own, W)


def solution(mesh):
    n, nx, nc = 8, 4, 2
    torus = Mesh(mesh.devices.reshape(n, n, nx, nc), (Z, Y, X, CORE))
    in_specs = (
        P(FS, None),
        P(None, FS, TP),
        P(None, FS, None),
        P(None, TP, None),
        P(None, FS, TP),
        P(None, FS, TP),
    )
    out_specs = (P(None, FS, TP), P(None, FS, TP), P(None, None, TP))
    return jax.shard_map(
        functools.partial(update, n, nx, nc),
        mesh=torus, in_specs=in_specs, out_specs=out_specs, check_vma=False)
```

time: 95.5 us -> 82.7 us (0.87)
  the two profiles are of different devices: /device:TPU:2 before, /device:TPU:8 now
where the time goes in v2:
time: 82.7 us; the launch traced here: 82.6 us
  Pallas kernels  81.9 us (99%)
    pallas_call x1, Pallas kernels, update(): pl.pallas_call(functools.partial(kernel, n, nx, nc, float(depth * W * nt)...  80.7 us

profile of v2, /device:TPU:8, one launch (start us, length us, event | category | flops | bytes accessed | tf_op | source)
XLA Modules:
  0.0 82.6 jit_solution(17024142384448911309)
XLA Ops:
  0.6 80.7 %update.1 = (f32[3,32,128]{2,1,0:T(8,128)S(1)}, f32[3,32,128]{2,1,0:T(8,128)S(1)}, bf16[3,8,8,2,16,128]{5,4,3,2,1,0:T(8,128)(2,1)S(1)}) custom-call(bf16[768,2048]{1,0:T(8,128)(2,1)} %x_hbm.1, bf16[3,768,128]{2,1,0:T(8,128)(2,1)} %c_hbm.1, f32[3,32,2048]{2,1,0:T(8,128)} %l_hbm.1, f32[3,128,128]{2,1,0:T(8,128)} %rr_hbm.1, f32[3,32,128]{2,1,0:T(8,128)} %mo_hbm.1, ...), custom_call_target="tpu_custom_call" | custom-call | tf_op jit(solution)/shard_map/update/pallas_call | solution.py:427
  81.4 1.2 %write_out.1 = (f32[3,32,128]{2,1,0:T(8,128)}, f32[3,32,128]{2,1,0:T(8,128)}, bf16[3,8,8,2,16,128]{5,4,3,2,1,0:T(8,128)(2,1)}) custom-call(f32[3,32,128]{2,1,0:T(8,128)S(1)} %get-tuple-element.9.refs_0_, f32[3,32,128]{2,1,0:T(8,128)S(1)} %get-tuple-element.10.refs_1_, bf16[3,8,8,2,16,128]{5,4,3,2,1,0:T(8,128)(2,1)S(1)} %get-tuple-element.11.refs_2_), custom_call_target="tpu_custom_call" | custom-call | tf_op jit(solution)/shard_map/write_out/pallas_call | solution.py:437

commit v3 on v2

--- a/solution.py
+++ b/solution.py
@@ -57,11 +57,23 @@
 
     barrier = pltpu.get_barrier_semaphore()
 
-    order = []
-    for k in range(half, 0, -1):
-        order.append(("L", k))
-        if k > 1:
-            order.append(("S", k - 1))
+    skip = half >= 2
+
+    def terms(chain, k):
+        top = half if chain == "L" else half - 1
+        if chain == "L" and skip:
+            if k >= half - 1:
+                return []
+            if k == half - 2:
+                return [half - 1, half]
+        return [k + 1] if k < top else []
+
+    def hop(chain, k):
+        return 2 if chain == "L" and skip and k == half else 1
+
+    order = [("L", half)]
+    for k in range(half - 1, 0, -1):
+        order += [("L", k), ("S", k)]
     order.append(("O", 0))
 
     def block_of(h, kind, k):
@@ -98,22 +110,21 @@
     for m in range(M):
         ct[m * W:(m + 1) * W, :] = cv[m].T
 
-    def ring_to(h, chain):
+    def ring_to(h, chain, links=1):
         name, b = big[h]
-        return {name: at(b + sgn) if chain == "L" else at(b - sgn)}
+        return {name: at(b + links * sgn) if chain == "L" else at(b - links * sgn)}
 
     def slot(chain, s):
         return s - 1 if chain == "L" else half + s - 1
 
     cp_rows = W // PARTS
 
-    def send_sum(h, chain, s, m, p):
-        k = half + 1 - s if chain == "L" else half - s
+    def send_sum(h, chain, k, m, p):
         rows = pl.ds(p * cp_rows, cp_rows)
         src = pb.at[h, block_of(h, chain, k), m, rows]
-        i = slot(chain, s)
+        i = slot(chain, k)
         remote(src, rb.at[h, i, m, rows], send_sem.at[0], rb_sem.at[h, i, m * PARTS + p],
-               ring_to(h, chain)).start()
+               ring_to(h, chain, hop(chain, k))).start()
 
     def got_sum(h, i, m, p):
         rows = pl.ds(p * cp_rows, cp_rows)
@@ -135,11 +146,11 @@
                     pb[h, block_of(h, kind, k), m] = piece.astype(BF16)
         if j == 0:
             pl.semaphore_wait(barrier, 2 * (n - 1) + nt - 1)
-        if (kind, k) == ("L", half) or (kind, k) == ("S", half - 1):
+        if kind != "O" and not terms(kind, k):
             for m in range(M):
                 for p in range(PARTS):
                     for h in range(2):
-                        send_sum(h, kind, 1, m, p)
+                        send_sum(h, kind, k, m, p)
 
     share = rows_own // nx
     part_rows = pl.ds(pl.multiple_of(x * share, share), share)
@@ -152,28 +163,29 @@
             remote(lv.at[:, part_rows, cols], lt.at[h, o - 1, :, part_rows, :], send_sem.at[8],
                    lt_sem.at[h, o - 1], {name: q}).start()
 
-    for s in range(2, half + 1):
+    for k in range(half - 1, 0, -1):
         for m in range(M):
             for p in range(PARTS):
                 rows = pl.ds(p * cp_rows, cp_rows)
-                for chain, last in (("L", half), ("S", half - 1)):
-                    if s > last:
+                for chain in ("L", "S"):
+                    if not terms(chain, k):
                         continue
-                    k = half + 1 - s if chain == "L" else half - s
                     for h in range(2):
-                        came = got_sum(h, slot(chain, s - 1), m, p)
                         b = block_of(h, chain, k)
-                        pb[h, b, m, rows] = (pb[h, b, m, rows].astype(F32) + came).astype(BF16)
-                        send_sum(h, chain, s, m, p)
+                        total = pb[h, b, m, rows].astype(F32)
+                        for far in terms(chain, k):
+                            total = total + got_sum(h, slot(chain, far), m, p)
+                        pb[h, b, m, rows] = total.astype(BF16)
+                        send_sum(h, chain, k, m, p)
 
     for m in range(M):
         for p in range(PARTS):
             rows = pl.ds(p * cp_rows, cp_rows)
             for h in range(2):
                 total = own[h, m, rows]
-                for chain, last in (("S", half - 1), ("L", half)):
-                    if last > 0:
-                        total = total + got_sum(h, slot(chain, last), m, p)
+                for chain in ("S", "L"):
+                    for far in terms(chain, 0):
+                        total = total + got_sum(h, slot(chain, far), m, p)
                 g1[h, m, rows] = total
                 s2[h, m, rows] = total.astype(BF16)
 
@@ -190,12 +202,6 @@
     for o in range(1, nx):
         mine = lt.at[:, :, :, part_rows, :]
         remote(mine, mine, send_sem.at[9], lx_sem.at[o - 1], {X: lax.rem(x + o, nx)}).start()
-    for h in range(2):
-        name, me = small[h]
-        ma_loads[h].wait()
-        for o in peers:
-            mine = mal.at[h, me]
-            remote(mine, mine, send_sem.at[3], ma_sem.at[h, o - 1], {name: at(me + o)}).start()
 
     def split_left(h, m, o, value):
         high = value.astype(BF16)
@@ -285,6 +291,12 @@
     sq2[z] = summed(sq1, n)
     for o in peers:
         remote(sq2.at[z], sq2.at[z], send_sem.at[4], sq_sem2.at[o - 1], {Z: at(z + o)}).start()
+    for h in range(2):
+        name, me = small[h]
+        ma_loads[h].wait()
+        for o in peers:
+            mine = mal.at[h, me]
+            remote(mine, mine, send_sem.at[3], ma_sem.at[h, o - 1], {name: at(me + o)}).start()
     for o in range(1, n):
         got(sq2.at[at(z - o)], sq_sem2.at[o - 1])
     sq3[t] = summed(sq2, n)
@@ -322,18 +334,24 @@
         return cp.at[m, part, b, 0] if h == 0 else cp.at[m, b, part, 1]
 
     def send_copy(h, chain, s, m, p):
-        ref = c_piece(h, held(h, chain, s - 1), m, p)
+        links = hop(chain, s)
+        ref = c_piece(h, held(h, chain, s - links), m, p)
         remote(ref, ref, send_sem.at[11 + h], cp_sem.at[h, slot(chain, s), m * PARTS + p],
-               ring_to(h, chain)).start()
+               ring_to(h, chain, links)).start()
+
+    def pass_on(h, chain, s, m, p):
+        last = half if chain == "L" else half - 1
+        for to in range(s + 1, last + 1):
+            if to - hop(chain, to) == s:
+                send_copy(h, chain, to, m, p)
 
     for m in range(M):
         for p in range(PARTS):
             for h in range(2):
                 make_copies(h, m, p)
             for h in range(2):
-                send_copy(h, "L", 1, m, p)
-                if half > 1:
-                    send_copy(h, "S", 1, m, p)
+                pass_on(h, "L", 0, m, p)
+                pass_on(h, "S", 0, m, p)
     for m in range(M):
         dirv[m] = mnv[m] * scales[m:m + 1, :]
     for s in range(1, half + 1):
@@ -345,8 +363,7 @@
                     for h in range(2):
                         got(c_piece(h, held(h, chain, s), m, p),
                             cp_sem.at[h, slot(chain, s), m * PARTS + p])
-                        if s < last:
-                            send_copy(h, chain, s + 1, m, p)
+                        pass_on(h, chain, s, m, p)
 
     got(rb, send_sem.at[0])
     got(r2, send_sem.at[1])

time: 82.7 us -> 81.3 us (0.983)
  the two profiles are of different devices: /device:TPU:8 before, /device:TPU:1 now
where the time goes in v3:
time: 81.3 us; the launch traced here: 81.2 us
  Pallas kernels  80.5 us (99%)
    pallas_call x1, Pallas kernels, update(): pl.pallas_call(functools.partial(kernel, n, nx, nc, float(depth * W * nt)...  79.4 us

profile of v3, /device:TPU:1, one launch (start us, length us, event | category | flops | bytes accessed | tf_op | source)
XLA Modules:
  0.0 81.2 jit_solution(13571320258139850714)
XLA Ops:
  0.6 79.4 %update.1 = (f32[3,32,128]{2,1,0:T(8,128)S(1)}, f32[3,32,128]{2,1,0:T(8,128)S(1)}, bf16[3,8,8,2,16,128]{5,4,3,2,1,0:T(8,128)(2,1)S(1)}) custom-call(bf16[768,2048]{1,0:T(8,128)(2,1)} %x_hbm.1, bf16[3,768,128]{2,1,0:T(8,128)(2,1)} %c_hbm.1, f32[3,32,2048]{2,1,0:T(8,128)} %l_hbm.1, f32[3,128,128]{2,1,0:T(8,128)} %rr_hbm.1, f32[3,32,128]{2,1,0:T(8,128)} %mo_hbm.1, ...), custom_call_target="tpu_custom_call" | custom-call | tf_op jit(solution)/shard_map/update/pallas_call | solution.py:444
  80.0 1.2 %write_out.1 = (f32[3,32,128]{2,1,0:T(8,128)}, f32[3,32,128]{2,1,0:T(8,128)}, bf16[3,8,8,2,16,128]{5,4,3,2,1,0:T(8,128)(2,1)}) custom-call(f32[3,32,128]{2,1,0:T(8,128)S(1)} %get-tuple-element.9.refs_0_, f32[3,32,128]{2,1,0:T(8,128)S(1)} %get-tuple-element.10.refs_1_, bf16[3,8,8,2,16,128]{5,4,3,2,1,0:T(8,128)(2,1)S(1)} %get-tuple-element.11.refs_2_), custom_call_target="tpu_custom_call" | custom-call | tf_op jit(solution)/shard_map/write_out/pallas_call | solution.py:454
